TPU v7x, 128 devices: a whole 4x4x4 slice. The times are simulated.
128 devices in a mesh: sp: 32 (over z, y, core), tp: 4 (over x).
Axes of the slice: x: 4, y: 4, z: 4, core: 2. Of those that a mesh axis runs over, the one named last changes fastest.
Arguments:
- residual_entry_input: bfloat16 [32768, 2048], P(('sp', 'tp')), may hold values from -6 to 6
- query_matrix_rows: bfloat16 [32768, 1024], P('sp', 'tp'), may hold values from -6 to 6
- key_matrix_rows: bfloat16 [32768, 1024], P('sp', 'tp'), may hold values from -6 to 6
- value_matrix_rows: bfloat16 [32768, 2048], P('sp', 'tp'), may hold values from -6 to 6
- output_gate_logits: bfloat16 [32768, 2048], P('sp', 'tp'), may hold values from -6 to 6
- input_gate_logits: float32 [32768, 8], P('sp', 'tp'), may hold values from -6 to 6
- forget_gate_logits: float32 [32768, 8], P('sp', 'tp'), may hold values from -8 to 31
- forget_decay_offset: float32 [32768, 8], P('sp', 'tp'), may hold values from -0.7 to 0
- head_norm_gain: float32 [8, 256], P('tp'), may hold values from 0.1 to 1.9
- cell_output_weight: bfloat16 [2048, 2048], P('tp'), may hold values from -0.125 to 0.125
- feedforward_norm_gain: float32 [2048], replicated, may hold values from 0.1 to 1.9
- gate_up_weight: bfloat16 [2048, 5632], P('sp', 'tp'), may hold values from -0.125 to 0.125
- value_up_weight: bfloat16 [2048, 5632], P('sp', 'tp'), may hold values from -0.125 to 0.125
- gate_filter_taps: float32 [3, 5632], P(None, 'tp'), may hold values from -3 to 3
- value_filter_taps: float32 [3, 5632], P(None, 'tp'), may hold values from -3 to 3
- down_projection_weight: bfloat16 [5632, 2048], P('tp', 'sp'), may hold values from -0.078125 to 0.078125
Outputs:
- result: bfloat16 [32768, 2048], P(('sp', 'tp'))
All inputs are finite; a program needn't handle non-finite values.
Results may differ from a plain program's by a relative error of at most 0.025.
Values may be sent and summed in bfloat16 or wider, within the bound.
A program may use at most 128 MiB of HBM per device.

v0:
```python
import jax
import jax.numpy as jnp
from jax import lax
from jax.sharding import Mesh
from jax.sharding import PartitionSpec as P

BLOCK = 128
SP = ("sp_0", "sp_1", "sp_2")
SP_TP = ("sp_0", "sp_1", "sp_2", "tp")
eps = 1e-06
neg_large = -1e30


def neutral_like(x, identity):
    return jax.tree.map(
        lambda part, zero: jnp.zeros_like(part) + jnp.asarray(zero, part.dtype), x, identity
    )


def gathered_once(x, axis):
    leaves = jax.tree.leaves(x)
    sequence = sorted(range(len(leaves)), key=lambda k: -leaves[k].size)
    width = (1, *leaves[sequence[0]].shape)[-1]
    lines = [
        jnp.pad(leaves[k].reshape(-1), (0, -leaves[k].size % width)).reshape(-1, width)
        for k in sequence
    ]
    both, at, found = (lax.all_gather(jnp.concatenate(lines), axis), 0, {})
    for k, line in zip(sequence, lines):
        slab = both[:, at : at + len(line)].reshape(len(both), -1)
        found[k] = slab[:, : leaves[k].size].reshape(-1, *leaves[k].shape)
        at += len(line)
    numbers = iter(range(len(leaves)))
    return jax.tree.map(lambda _: found[next(numbers)], x)


def entering(x, axes, combine, identity):
    before = start = neutral_like(x, identity)
    running = x
    for axis in reversed(axes):
        count, position = (lax.axis_size(axis), lax.axis_index(axis))
        pieces = gathered_once(
            jax.tree.map(
                lambda part, kind: part.astype(kind),
                running,
                (jnp.bfloat16, jnp.bfloat16, jnp.bfloat16, jnp.bfloat16),
            ),
            axis,
        )
        inside, running = (start, start)
        for k in range(count):
            passed = k < position
            running = combine(
                running, jax.tree.map(lambda part, own: part[k].astype(own.dtype), pieces, x)
            )
            inside = jax.tree.map(lambda new, old: jnp.where(passed, new, old), running, inside)
        before = combine(inside, before)
    return before


def shifted(x, axis, by):
    count = lax.axis_size(axis)
    pairs = [(i, i + by) for i in range(count) if 0 <= i + by < count]
    return lax.ppermute(x, axis, pairs)


def side_by_side(arrays, axis, dim, along):
    both = jnp.concatenate(arrays, axis=along)
    result, at, finished = (lax.all_gather(both, axis, axis=dim, tiled=True), 0, [])
    for a in arrays:
        finished.append(lax.slice_in_dim(result, at, at + a.shape[along], axis=along))
        at += a.shape[along]
    return tuple(finished)


def laid_out(tiles, dim):
    shape = list(tiles.shape[1:])
    shape[dim] *= tiles.shape[0]
    return jnp.moveaxis(tiles, 0, dim).reshape(shape)


def all_blocks(x, axes, sequence):
    tiles = x
    for k in sequence:
        tiles = lax.all_gather(tiles, axes[k])
    done = sequence[::-1]
    back = [done.index(k) for k in range(len(axes))]
    tiles = tiles.transpose(*back, *range(len(axes), tiles.ndim))
    return tiles.reshape(-1, *x.shape)


def gather_axes(x, axes, sequence, dim):
    return laid_out(all_blocks(x, axes, sequence), dim)


def gate_log_values(input_gate_logits, forget_gate_logits, forget_decay_offset):
    input_log_value = 15.0 * jnp.tanh(input_gate_logits / 15.0)
    forget_log_sigmoid = (
        jax.nn.log_sigmoid(15.0 * jnp.tanh(forget_gate_logits / 15.0)) + forget_decay_offset
    )
    return (input_log_value, forget_log_sigmoid)


def combine_states(earlier, later):
    total_one, memory_one, normer_one, running_one = earlier
    total_two, memory_two, normer_two, running_two = later
    joined = jnp.maximum(total_two + running_one, running_two)
    weight_one = jnp.exp(total_two + running_one - joined)
    weight_two = jnp.exp(running_two - joined)
    memory = weight_one[:, None, None] * memory_one + weight_two[:, None, None] * memory_two
    normer = weight_one[:, None] * normer_one + weight_two[:, None] * normer_two
    return (total_one + total_two, memory, normer, joined)


def local_step(state_carry, inputs):
    memory, normer, running = state_carry
    query_block, key_block, value_block, input_block, forget_block = inputs
    length = query_block.shape[0]
    highest = lax.Precision.DEFAULT
    query_scale = query_block.shape[2] ** (-0.5)
    causal = jnp.tril(jnp.ones((length, length), dtype=bool))[:, :, None]
    cumulative = jnp.cumsum(forget_block, axis=0)
    logits = cumulative[:, None, :] - cumulative[None, :, :] + input_block[None, :, :]
    logits = jnp.where(causal, logits, -jnp.inf)
    carried = cumulative + running[None, :]
    stable = jnp.maximum(carried, jnp.max(logits, axis=1))
    carry_weight = jnp.exp(carried - stable)
    raw = (
        jnp.einsum("thd,shd->tsh", query_block, key_block, preferred_element_type=jnp.float32)
        * query_scale
    )
    scores = raw * jnp.exp(logits - stable[:, None, :])
    scaled_query = query_block.astype(jnp.float32) * query_scale
    numerator = carry_weight[:, :, None] * jnp.einsum(
        "hvd,thd->thv", memory, scaled_query, precision=highest
    )
    numerator = numerator + jnp.einsum(
        "tsh,shv->thv", scores.astype(jnp.bfloat16), value_block, preferred_element_type=jnp.float32
    )
    denominator = carry_weight * jnp.einsum(
        "hd,thd->th", normer, scaled_query, precision=highest
    ) + jnp.sum(scores, axis=1)
    last_sum = cumulative[-1]
    weights_log = last_sum[None, :] - cumulative + input_block
    new_running = jnp.maximum(last_sum + running, jnp.max(weights_log, axis=0))
    decay_factor = jnp.exp(last_sum + running - new_running)
    weighted = (
        key_block.astype(jnp.float32) * jnp.exp(weights_log - new_running[None, :])[:, :, None]
    )
    memory = decay_factor[:, None, None] * memory + jnp.einsum(
        "shv,shd->hvd",
        value_block,
        weighted.astype(jnp.bfloat16),
        preferred_element_type=jnp.float32,
    )
    normer = decay_factor[:, None] * normer + jnp.sum(weighted, axis=0)
    return ((memory, normer, new_running), (numerator, denominator, stable))


def local(
    residual_entry_input,
    query_matrix_rows,
    key_matrix_rows,
    value_matrix_rows,
    output_gate_logits,
    input_gate_logits,
    forget_gate_logits,
    forget_decay_offset,
    head_norm_gain,
    cell_output_weight,
    feedforward_norm_gain,
    gate_up_weight,
    value_up_weight,
    gate_filter_taps,
    value_filter_taps,
    down_projection_weight,
):
    highest = lax.Precision.DEFAULT
    token_count = query_matrix_rows.shape[0]
    head_count = input_gate_logits.shape[1]
    key_width = query_matrix_rows.shape[1] // head_count
    value_width = value_matrix_rows.shape[1] // head_count
    query_scale = key_width ** (-0.5)
    queries_low = query_matrix_rows.reshape(token_count, head_count, key_width)
    keys_low = key_matrix_rows.reshape(token_count, head_count, key_width)
    values_low = value_matrix_rows.reshape(token_count, head_count, value_width)
    input_log_value, forget_log_sigmoid = gate_log_values(
        input_gate_logits, forget_gate_logits, forget_decay_offset
    )
    cumulative = jnp.cumsum(forget_log_sigmoid, axis=0)
    total_log = cumulative[-1]
    block_count = token_count // BLOCK

    def blocks(tensor):
        return tensor.reshape((block_count, BLOCK) + tensor.shape[1:])

    initial = (
        jnp.zeros((head_count, value_width, key_width), jnp.float32),
        jnp.zeros((head_count, key_width), jnp.float32),
        jnp.full((head_count,), neg_large, jnp.float32),
    )
    end_state, (numerator, denominator, stable) = lax.scan(
        local_step,
        initial,
        (
            blocks(queries_low),
            blocks(keys_low),
            blocks(values_low),
            blocks(input_log_value),
            blocks(forget_log_sigmoid),
        ),
    )
    end_memory, end_normer, end_running = end_state
    identity = (
        jnp.zeros((head_count,), jnp.float32),
        jnp.zeros((head_count, value_width, key_width), jnp.float32),
        jnp.zeros((head_count, key_width), jnp.float32),
        jnp.full((head_count,), neg_large, jnp.float32),
    )
    prefix = entering(
        (total_log, end_memory, end_normer, end_running), SP, combine_states, identity
    )
    numerator = numerator.reshape(token_count, head_count, value_width)
    denominator = denominator.reshape(token_count, head_count)
    stable = stable.reshape(token_count, head_count)
    _, prior_memory, prior_normer, prior_running = prefix
    scaled_query = queries_low.astype(jnp.float32) * query_scale
    prior_log = cumulative + prior_running[None, :]
    top_log = jnp.maximum(stable, prior_log)
    local_weight = jnp.exp(stable - top_log)
    prior_weight = jnp.exp(prior_log - top_log)
    numerator = local_weight[:, :, None] * numerator + prior_weight[:, :, None] * jnp.einsum(
        "hvd,thd->thv", prior_memory, scaled_query, precision=highest
    )
    denominator = local_weight * denominator + prior_weight * jnp.einsum(
        "hd,thd->th", prior_normer, scaled_query, precision=highest
    )
    memory_out = numerator / jnp.maximum(jnp.abs(denominator), jnp.exp(-top_log))[:, :, None]
    normed = (
        memory_out
        * lax.rsqrt(jnp.mean(memory_out * memory_out, axis=-1, keepdims=True) + eps)
        * head_norm_gain[None, :, :]
    )
    gated_rows = (
        normed.reshape(token_count, head_count * value_width)
        * jax.nn.sigmoid(output_gate_logits.astype(jnp.float32))
    ).astype(jnp.bfloat16)
    whole_out = lax.all_gather(cell_output_weight, "tp", axis=0, tiled=True)
    own_rows = lax.all_to_all(gated_rows, "tp", split_axis=0, concat_axis=1, tiled=True)
    mixed_rows = jnp.dot(own_rows, whole_out, preferred_element_type=jnp.float32)
    stream_wide = residual_entry_input.astype(jnp.float32) + mixed_rows
    stream = stream_wide.astype(jnp.bfloat16)
    stream_wide = lax.optimization_barrier(stream).astype(jnp.float32)
    normed_rows = (
        stream_wide
        * lax.rsqrt(jnp.mean(stream_wide * stream_wide, axis=-1, keepdims=True) + eps)
        * feedforward_norm_gain[None, :]
    ).astype(jnp.bfloat16)
    group_rows = lax.all_gather(normed_rows, "tp", axis=0, tiled=True)
    earlier_rows = shifted(group_rows[-2:], SP, 1)
    window = jnp.concatenate([earlier_rows, group_rows], axis=0)
    pieces = side_by_side((gate_up_weight, value_up_weight), SP, 0, 1)
    up_gate = jnp.dot(window, pieces[0], preferred_element_type=jnp.float32)
    up_value = jnp.dot(window, pieces[1], preferred_element_type=jnp.float32)
    conv_g = (
        gate_filter_taps[0][None, :] * up_gate[:-2]
        + gate_filter_taps[1][None, :] * up_gate[1:-1]
        + gate_filter_taps[2][None, :] * up_gate[2:]
    )
    conv_v = (
        value_filter_taps[0][None, :] * up_value[:-2]
        + value_filter_taps[1][None, :] * up_value[1:-1]
        + value_filter_taps[2][None, :] * up_value[2:]
    )
    hidden = (jax.nn.silu(conv_g) * conv_v).astype(jnp.bfloat16)
    whole_down = gather_axes(down_projection_weight, (("sp_0", "sp_1"), "sp_2"), (0, 1), 1)
    ffn_rows = lax.psum_scatter(
        jnp.dot(hidden, whole_down, preferred_element_type=jnp.float32).astype(jnp.bfloat16),
        "tp",
        scatter_dimension=0,
        tiled=True,
    ).astype(jnp.float32)
    return (stream_wide + ffn_rows).astype(jnp.bfloat16)


def solution(mesh):
    split = Mesh(mesh.devices.reshape(4, 4, 2, mesh.shape["tp"]), ("sp_0", "sp_1", "sp_2", "tp"))
    placed = (
        P(SP_TP, None),
        P(SP, "tp"),
        P(SP, "tp"),
        P(SP, "tp"),
        P(SP, "tp"),
        P(SP, "tp"),
        P(SP, "tp"),
        P(SP, "tp"),
        P("tp", None),
        P("tp", None),
        P(),
        P(SP, "tp"),
        P(SP, "tp"),
        P(None, "tp"),
        P(None, "tp"),
        P("tp", SP),
    )
    return jax.shard_map(
        local, mesh=split, in_specs=placed, out_specs=P(SP_TP, None), check_vma=False
    )
```

profile of v0, /device:TPU:1, one launch (start us, length us, event | category | flops | bytes accessed | tf_op | source)
XLA Modules:
  0.0 419.1 jit_solution(10256180526580571442)
XLA Ops:
  13.6 102.5 %while.21 = (s32[]{:T(128)}, f32[2,256,128]{2,1,0:T(8,128)S(1)}, f32[2,128]{1,0:T(2,128)S(1)}, f32[2]{0:T(128)S(1)}, f32[8,128,2,256]{1,0,3,2:T(8,128)}, /*index...) while((s32[]{:T(128)}, f32[2,256,128]{2,1,0:T(8,128)S(1)}, ...), condition=%wide.region_6.7_spmd.clone, body=%wide.region_0.6_spmd.clone.sunk | while | flops 59952648 | bytes 4685610 | solution.py:202
  17.8 8.3 %dynamic_update_slice.19 = f32[8,128,2,256]{1,0,3,2:T(8,128)} dynamic-update-slice(f32[8,128,2,256]{1,0,3,2:T(8,128)} %get-tuple-element.428, f32[1,128,2,256]{1,0,3,2:T(1,128)S(1)} %copy.336, s32[]{:T(128)} %get-tuple-element.424, s32[]{:T(128)} %constant.38.clone.1..sunk, s32[]{:T(128)} %constant.38.clone.1..sunk, s32[]{:T(128)} %constant.38.clone.1..sunk) | dynamic-update-slice | bytes 524292 | tf_op jit(solution)/shard_map/while/body/jit(dynamic_update_index_in_dim)/dynamic_update_slice | solution.py:202
  30.7 8.2 %dynamic_update_slice.19 = f32[8,128,2,256]{1,0,3,2:T(8,128)} dynamic-update-slice(f32[8,128,2,256]{1,0,3,2:T(8,128)} %get-tuple-element.428, f32[1,128,2,256]{1,0,3,2:T(1,128)S(1)} %copy.336, s32[]{:T(128)} %get-tuple-element.424, s32[]{:T(128)} %constant.38.clone.1..sunk, s32[]{:T(128)} %constant.38.clone.1..sunk, s32[]{:T(128)} %constant.38.clone.1..sunk) | dynamic-update-slice | bytes 524292 | tf_op jit(solution)/shard_map/while/body/jit(dynamic_update_index_in_dim)/dynamic_update_slice | solution.py:202
  43.5 8.2 %dynamic_update_slice.19 = f32[8,128,2,256]{1,0,3,2:T(8,128)} dynamic-update-slice(f32[8,128,2,256]{1,0,3,2:T(8,128)} %get-tuple-element.428, f32[1,128,2,256]{1,0,3,2:T(1,128)S(1)} %copy.336, s32[]{:T(128)} %get-tuple-element.424, s32[]{:T(128)} %constant.38.clone.1..sunk, s32[]{:T(128)} %constant.38.clone.1..sunk, s32[]{:T(128)} %constant.38.clone.1..sunk) | dynamic-update-slice | bytes 524292 | tf_op jit(solution)/shard_map/while/body/jit(dynamic_update_index_in_dim)/dynamic_update_slice | solution.py:202
  56.3 8.2 %dynamic_update_slice.19 = f32[8,128,2,256]{1,0,3,2:T(8,128)} dynamic-update-slice(f32[8,128,2,256]{1,0,3,2:T(8,128)} %get-tuple-element.428, f32[1,128,2,256]{1,0,3,2:T(1,128)S(1)} %copy.336, s32[]{:T(128)} %get-tuple-element.424, s32[]{:T(128)} %constant.38.clone.1..sunk, s32[]{:T(128)} %constant.38.clone.1..sunk, s32[]{:T(128)} %constant.38.clone.1..sunk) | dynamic-update-slice | bytes 524292 | tf_op jit(solution)/shard_map/while/body/jit(dynamic_update_index_in_dim)/dynamic_update_slice | solution.py:202
  69.1 8.2 %dynamic_update_slice.19 = f32[8,128,2,256]{1,0,3,2:T(8,128)} dynamic-update-slice(f32[8,128,2,256]{1,0,3,2:T(8,128)} %get-tuple-element.428, f32[1,128,2,256]{1,0,3,2:T(1,128)S(1)} %copy.336, s32[]{:T(128)} %get-tuple-element.424, s32[]{:T(128)} %constant.38.clone.1..sunk, s32[]{:T(128)} %constant.38.clone.1..sunk, s32[]{:T(128)} %constant.38.clone.1..sunk) | dynamic-update-slice | bytes 524292 | tf_op jit(solution)/shard_map/while/body/jit(dynamic_update_index_in_dim)/dynamic_update_slice | solution.py:202
  81.9 8.2 %dynamic_update_slice.19 = f32[8,128,2,256]{1,0,3,2:T(8,128)} dynamic-update-slice(f32[8,128,2,256]{1,0,3,2:T(8,128)} %get-tuple-element.428, f32[1,128,2,256]{1,0,3,2:T(1,128)S(1)} %copy.336, s32[]{:T(128)} %get-tuple-element.424, s32[]{:T(128)} %constant.38.clone.1..sunk, s32[]{:T(128)} %constant.38.clone.1..sunk, s32[]{:T(128)} %constant.38.clone.1..sunk) | dynamic-update-slice | bytes 524292 | tf_op jit(solution)/shard_map/while/body/jit(dynamic_update_index_in_dim)/dynamic_update_slice | solution.py:202
  94.7 8.2 %dynamic_update_slice.19 = f32[8,128,2,256]{1,0,3,2:T(8,128)} dynamic-update-slice(f32[8,128,2,256]{1,0,3,2:T(8,128)} %get-tuple-element.428, f32[1,128,2,256]{1,0,3,2:T(1,128)S(1)} %copy.336, s32[]{:T(128)} %get-tuple-element.424, s32[]{:T(128)} %constant.38.clone.1..sunk, s32[]{:T(128)} %constant.38.clone.1..sunk, s32[]{:T(128)} %constant.38.clone.1..sunk) | dynamic-update-slice | bytes 524292 | tf_op jit(solution)/shard_map/while/body/jit(dynamic_update_index_in_dim)/dynamic_update_slice | solution.py:202
  107.5 8.2 %dynamic_update_slice.19 = f32[8,128,2,256]{1,0,3,2:T(8,128)} dynamic-update-slice(f32[8,128,2,256]{1,0,3,2:T(8,128)} %get-tuple-element.428, f32[1,128,2,256]{1,0,3,2:T(1,128)S(1)} %copy.336, s32[]{:T(128)} %get-tuple-element.424, s32[]{:T(128)} %constant.38.clone.1..sunk, s32[]{:T(128)} %constant.38.clone.1..sunk, s32[]{:T(128)} %constant.38.clone.1..sunk) | dynamic-update-slice | bytes 524292 | tf_op jit(solution)/shard_map/while/body/jit(dynamic_update_index_in_dim)/dynamic_update_slice | solution.py:202
  117.4 3.0 all-gather.5
  122.3 13.0 %all-gather.6 = bf16[4,516,128]{2,1,0:T(8,128)(2,1)S(1)} all-gather(bf16[1,516,128]{2,1,0:T(8,128)(2,1)S(1)} %maximum_bitcast_fusion.1), channel_id=3, replica_groups=mesh['sp_0'=4,'sp_1'=4,'sp_2'=2,'tp'=4] {'sp_1'}, dimensions={0}, use_global_device_ids=true | all-gather | bytes 660480 | tf_op jit(solution)/shard_map/all_gather | solution.py:28
  136.8 14.1 %all-gather.7 = bf16[4,516,128]{2,1,0:T(8,128)(2,1)S(1)} all-gather(bf16[1,516,128]{2,1,0:T(8,128)(2,1)S(1)} %maximum_bitcast_fusion.2), channel_id=4, replica_groups=mesh['sp_0'=4,'sp_1'=4,'sp_2'=2,'tp'=4] {'sp_0'}, dimensions={0}, use_global_device_ids=true | all-gather | bytes 660480 | tf_op jit(solution)/shard_map/all_gather | solution.py:28
  161.7 14.4 %all_to_all.19 = bf16[4,256,512]{2,1,0:T(8,128)(2,1)S(1)} all-to-all(bf16[4,256,512]{2,1,0:T(8,128)(2,1)S(1)} %bitcast.610), channel_id=1, replica_groups=mesh['sp_0'=4,'sp_1'=4,'sp_2'=2,'tp'=4] {'tp'}, dimensions={0} | all-to-all | bytes 2097152 | tf_op jit(solution)/shard_map/all_to_all | solution.py:249
  176.6 5.7 %fusion.40 = bf16[256,2048]{1,0:T(8,128)(2,1)S(1)} fusion(bf16[256,2048]{0,1:T(8,128)(2,1)S(1)} %bitcast.606, bf16[2048,2048]{1,0:T(8,128)(2,1)} %all-gather.14.cloned.1.call-done, bf16[256,2048]{1,0:T(8,128)(2,1)S(1)} %copy-done), kind=kOutput, calls=%fused_computation.77 | convolution fusion | flops 2149056512 | bytes 11534336 | tf_op jit(solution)/shard_map/dot_general | solution.py:250
  184.1 3.8 copy.246
  188.9 45.1 %all-gather.16.cloned.1.call-done = bf16[1024,2048]{1,0:T(8,128)(2,1)} async-done(((bf16[256,2048]{1,0:T(8,128)(2,1)}), bf16[1024,2048]{1,0:T(8,128)(2,1)}) %all-gather.16.cloned.1.call-update) | async-done | bytes 4194320 | tf_op jit(solution)/shard_map/all_gather | solution.py:259
  234.8 4.0 collective-permute-start
  238.9 16.3 %all-gather.22.cloned.1.call-done = bf16[32,1408,64]{1,0,2:T(8,128)(2,1)} async-done(((bf16[16,1408,64]{1,0,2:T(8,128)(2,1)}), bf16[32,1408,64]{1,0,2:T(8,128)(2,1)}) %all-gather.22.cloned.1.call-update) | async-done | bytes 5767184 | tf_op jit(solution)/shard_map/all_gather | solution.py:85
  255.2 7.0 %copy.200 = bf16[16,2,1408,64]{2,3,1,0:T(8,128)(2,1)} copy(bf16[16,2,1408,64]{2,0,1,3:T(8,128)(2,1)} %bitcast.607) | data formatting | bytes 11534336 | tf_op jit(solution)/shard_map/transpose | solution.py:88
  262.2 56.7 %all-gather.18.cloned.1.call-done = bf16[2048,2816]{1,0:T(8,128)(2,1)} async-done(((bf16[64,2816]{1,0:T(8,128)(2,1)}), bf16[2048,2816]{1,0:T(8,128)(2,1)}) %all-gather.18.cloned.1.call-update) | async-done | bytes 11534352 | tf_op jit(solution)/shard_map/all_gather | solution.py:69
  318.9 11.9 %fusion.37 = f32[1026,1408]{1,0:T(8,128)} fusion(bf16[2048,2816]{1,0:T(8,128)(2,1)} %all-gather.18.cloned.1.call-done, bf16[1024,2048]{1,0:T(8,128)(2,1)} %all-gather.16.cloned.1.call-done, bf16[2,2048]{1,0:T(2,128)(2,1)S(1)} %collective-permute-done), kind=kOutput, calls=%fused_computation.69 | convolution fusion | flops 5925519360 | bytes 15748096 | tf_op jit(solution)/shard_map/dot_general | solution.py:263
  330.9 8.7 %fusion.33 = f32[1026,1408]{1,0:T(8,128)} fusion(bf16[2048,2816]{1,0:T(8,128)(2,1)S(1)} %copy-done.13, bf16[1024,2048]{1,0:T(8,128)(2,1)S(1)} %copy-done.12, bf16[2,2048]{1,0:T(2,128)(2,1)S(1)} %collective-permute-done), kind=kOutput, calls=%fused_computation.62 | convolution fusion | flops 5925519360 | bytes 15748096 | tf_op jit(solution)/shard_map/dot_general | solution.py:264
  339.5 24.1 %convolution_convert_fusion = bf16[1024,2048]{1,0:T(8,128)(2,1)} fusion(bf16[1408,2048]{0,1:T(8,128)(2,1)} %bitcast.608, f32[1026,1408]{1,0:T(8,128)} %fusion.33, f32[1026,1408]{1,0:T(8,128)} %fusion.37, f32[1408]{0:T(1024)S(1)} %get-tuple-element.181, f32[1408]{0:T(1024)S(1)} %get-tuple-element.182, f32[1408]{0:T(1024)S(1)} %get-tuple-element.180, ...), kind=kOutput, calls=%fused_computation.72 | convolution fusion | flops 5930745856 | bytes 44598272 | tf_op jit(solution)/shard_map/dot_general | solution.py:278
  363.7 46.0 %reduce-scatter.2.cloned.1.call-done = bf16[256,2048]{1,0:T(8,128)(2,1)} async-done(((bf16[1024,2048]{1,0:T(8,128)(2,1)}), bf16[256,2048]{1,0:T(8,128)(2,1)}) %reduce-scatter.2.cloned.1.call-update) | async-done | bytes 1048592 | tf_op jit(solution)/shard_map/reduce_scatter | solution.py:277
  (365 shorter events, 64.2 us)
Async XLA Ops:
  6.5 3.9 copy-start.10
  6.5 4.2 copy-start.1
  6.5 170.0 %all-gather.14.cloned.1.call-start = ((), (), s32[]{:S(2)}) async-start(), calls=%async_computation.2 | async-start | bytes 10485760 | tf_op jit(solution)/shard_map/all_gather | solution.py:248
  7.3 176.8 %all-gather.20.cloned.1.call-start = ((), (), s32[]{:S(2)}) async-start(), calls=%async_computation.6 | async-start | bytes 3063808 | tf_op jit(solution)/shard_map/all_gather | solution.py:85
  8.0 226.0 %all-gather.16.cloned.1.call-start = ((), (), s32[]{:S(2)}) async-start(), calls=%async_computation.3 | async-start | bytes 5242880 | tf_op jit(solution)/shard_map/all_gather | solution.py:259
  116.1 34.9 %copy-start.4 = (f32[8,128,2]{2,1,0:T(8,128)S(1)}, f32[8,128,2]{2,1,0:T(8,128)}, u32[]{:S(2)}) copy-start(f32[8,128,2]{2,1,0:T(8,128)} %get-tuple-element.72) | copy-start | bytes 24580
  116.1 35.1 %copy-start.3 = (f32[8,128,2]{2,1,0:T(8,128)S(1)}, f32[8,128,2]{2,1,0:T(8,128)}, u32[]{:S(2)}) copy-start(f32[8,128,2]{2,1,0:T(8,128)} %get-tuple-element.77) | copy-start | bytes 24580
  153.1 2.6 copy-start.2
  155.7 1.3 copy-start.11
  159.2 17.4 %copy-start = (bf16[256,2048]{1,0:T(8,128)(2,1)S(1)}, bf16[256,2048]{1,0:T(8,128)(2,1)}, u32[]{:S(2)}) copy-start(bf16[256,2048]{1,0:T(8,128)(2,1)} %param.18) | copy-start | bytes 3145732
  176.6 6.0 %copy-start.9 = (f32[2048]{0:T(1024)S(1)}, f32[2048]{0:T(1024)}, u32[]{:S(2)}) copy-start(f32[2048]{0:T(1024)} %param.28) | copy-start | bytes 24580
  184.0 71.2 %all-gather.22.cloned.1.call-start = ((), (), s32[]{:S(2)}) async-start(), calls=%async_computation.7 | async-start | bytes 8650752 | tf_op jit(solution)/shard_map/all_gather | solution.py:85
  184.0 4.0 copy-start.5
  184.0 4.0 copy-start.6
  184.1 54.8 %copy-start.7 = (f32[3,1408]{1,0:T(4,128)S(1)}, f32[3,1408]{1,0:T(4,128)}, u32[]{:S(2)}) copy-start(f32[3,1408]{1,0:T(4,128)} %param.32) | copy-start | bytes 50692
  184.1 54.8 %copy-start.8 = (f32[3,1408]{1,0:T(4,128)S(1)}, f32[3,1408]{1,0:T(4,128)}, u32[]{:S(2)}) copy-start(f32[3,1408]{1,0:T(4,128)} %param.31) | copy-start | bytes 50692
  187.9 131.0 %all-gather.18.cloned.1.call-start = ((), (), s32[]{:S(2)}) async-start(), calls=%async_computation.4 | async-start | bytes 11894784 | tf_op jit(solution)/shard_map/all_gather | solution.py:69
  188.8 220.8 %reduce-scatter.2.cloned.1.call-start = ((), (), s32[]{:S(2)}) async-start(), calls=%async_computation.5 | async-start | bytes 5242880 | tf_op jit(solution)/shard_map/reduce_scatter | solution.py:277
  234.8 27.4 %collective-permute-start = (bf16[2,2048]{1,0:T(2,128)(2,1)S(1)}, bf16[2,2048]{1,0:T(2,128)(2,1)S(1)}, u32[]{:S(2)}, u32[]{:S(2)}) collective-permute-start(bf16[2,2048]{1,0:T(2,128)(2,1)S(1)} %slice.352), channel_id=1, source_target_pairs={{0,4},{4,8},{8,12},{12,16},{16,20},{20,24},{24,28},{28,32},{32,36}... | collective-permute-start | bytes 24584 | tf_op jit(solution)/shard_map/ppermute | solution.py:64
  318.9 11.9 %copy-start.12 = (bf16[1024,2048]{1,0:T(8,128)(2,1)S(1)}, bf16[1024,2048]{1,0:T(8,128)(2,1)}, u32[]{:S(2)}) copy-start(bf16[1024,2048]{1,0:T(8,128)(2,1)} %all-gather.16.cloned.1.call-done) | copy-start | bytes 12582916
  318.9 11.9 %copy-start.13 = (bf16[2048,2816]{1,0:T(8,128)(2,1)S(1)}, bf16[2048,2816]{1,0:T(8,128)(2,1)}, u32[]{:S(2)}) copy-start(bf16[2048,2816]{1,0:T(8,128)(2,1)} %all-gather.18.cloned.1.call-done) | copy-start | bytes 34603012
Sparse Core Ops, SparseCore 0:
  9.0 86.0 all-gather.13
  97.3 51.0 all-gather.19
  184.1 49.8 all-gather.15
  235.5 19.6 all-gather.21
  257.3 61.5 all-gather.17
  363.8 45.7 reduce-scatter.1
where the time goes:
time: 421 us; the launch traced here: 419 us
  waiting for transfers between devices  166 us (39%)
  local copies, waits for them, and re-layouts  105 us (25%)
  matrix products  62 us (15%)
  blocking collectives  44.6 us (11%)
  other arithmetic  23.2 us (6%)
  between operations  14.1 us (3%)
  starting transfers between devices  4.22 us (1%)
    dynamic_update_slice x16, local copies, waits for them, and re-layouts, local(): lax.scan(local_step, initial, (blocks(queries_low), blocks(keys_low), blo...  66.9 us
    all_gather x1, waiting for transfers between devices, side_by_side(): lax.all_gather(both, axis, axis=dim, tiled=True)  56.7 us
    reduce_scatter x1, waiting for transfers between devices, local(): lax.psum_scatter(jnp.dot(hidden, whole_down, preferred_element_type=jnp.f...  46 us
    all_gather x1, waiting for transfers between devices, local(): group_rows = lax.all_gather(normed_rows, 'tp', axis=0, tiled=True)  45.1 us
    all_gather x3, blocking collectives, gathered_once(): both, at, found = (lax.all_gather(jnp.concatenate(lines), axis), 0, {})  30.2 us
    dot_general x1, matrix products, local(): jnp.dot(hidden, whole_down, preferred_element_type=jnp.float32)  24.1 us
    all_gather x2, waiting for transfers between devices, all_blocks(): tiles = lax.all_gather(tiles, axes[k])  16.3 us
    all_to_all x1, blocking collectives, local(): lax.all_to_all(gated_rows, 'tp', split_axis=0, concat_axis=1, tiled=True)  14.4 us
  transfers between devices with their start and end apart: 7, of which 4 were waited for; matrix products, arithmetic and copies ran while one was open for 34% of the time, Pallas kernels for 0%

commit v1 on v0

--- a/solution.py
+++ b/solution.py
@@ -256,7 +256,9 @@
         * lax.rsqrt(jnp.mean(stream_wide * stream_wide, axis=-1, keepdims=True) + eps)
         * feedforward_norm_gain[None, :]
     ).astype(jnp.bfloat16)
-    group_rows = lax.all_gather(normed_rows, "tp", axis=0, tiled=True)
+    group_rows = jnp.concatenate(
+        lax.all_to_all(jnp.stack(lax.axis_size("tp") * [normed_rows], axis=0), "tp", 0, 0), axis=0
+    )
     earlier_rows = shifted(group_rows[-2:], SP, 1)
     window = jnp.concatenate([earlier_rows, group_rows], axis=0)
     pieces = side_by_side((gate_up_weight, value_up_weight), SP, 0, 1)

time: 421 us -> 398 us (0.945)
  waiting for transfers between devices: 166 us -> 97.6 us
  blocking collectives: 44.6 us -> 85.4 us
  starting transfers between devices: 4.22 us -> 10.2 us
    all_gather x1, waiting for transfers between devices: 56.7 us -> 0.01 us  [side_by_side(): lax.all_gather(both, axis, axis=dim, tiled=True)]
    all_gather x1 -> x0, waiting for transfers between devices: 45.1 us -> none  [local(): group_rows = lax.all_gather(normed_rows, 'tp', axis=0, tiled=True)]
    all_to_all x0 -> x1, blocking collectives: none -> 44.8 us  [local(): lax.all_to_all(jnp.stack(lax.axis_size('tp') * [normed_rows], axis=0), 't...]
    all_gather x2, waiting for transfers between devices: 16.3 us -> 51.1 us  [all_blocks(): tiles = lax.all_gather(tiles, axes[k])]
    ppermute x1, starting transfers between devices: 4.02 us -> 10.1 us  [shifted(): return lax.ppermute(x, axis, pairs)]
  transfers between devices with their start and end apart: 7 -> 6, of which waited for: 4 -> 2; matrix products, arithmetic and copies ran while one was open for 34% -> 35% of each run, Pallas kernels for 0% -> 0%
where the time goes in v1:
time: 398 us; the launch traced here: 396 us
  local copies, waits for them, and re-layouts  106 us (27%)
  waiting for transfers between devices  97.6 us (25%)
  blocking collectives  85.4 us (21%)
  matrix products  60.7 us (15%)
  other arithmetic  21.6 us (5%)
  between operations  13.7 us (3%)
  starting transfers between devices  10.2 us (3%)
    dynamic_update_slice x16, local copies, waits for them, and re-layouts, local(): lax.scan(local_step, initial, (blocks(queries_low), blocks(keys_low), blo...  66.7 us
    all_gather x2, waiting for transfers between devices, all_blocks(): tiles = lax.all_gather(tiles, axes[k])  51.1 us
    reduce_scatter x1, waiting for transfers between devices, local(): lax.psum_scatter(jnp.dot(hidden, whole_down, preferred_element_type=jnp.f...  45 us
    all_to_all x1, blocking collectives, local(): lax.all_to_all(jnp.stack(lax.axis_size('tp') * [normed_rows], axis=0), 't...  44.8 us
    all_gather x3, blocking collectives, gathered_once(): both, at, found = (lax.all_gather(jnp.concatenate(lines), axis), 0, {})  26.2 us
    dot_general x1, matrix products, local(): jnp.dot(hidden, whole_down, preferred_element_type=jnp.float32)  22.6 us
    all_to_all x1, blocking collectives, local(): lax.all_to_all(gated_rows, 'tp', split_axis=0, concat_axis=1, tiled=True)  14.4 us
    dot_general x1, matrix products, local(): up_gate = jnp.dot(window, pieces[0], preferred_element_type=jnp.float32)  11.9 us
  transfers between devices with their start and end apart: 6, of which 2 were waited for; matrix products, arithmetic and copies ran while one was open for 35% of the time, Pallas kernels for 0%

profile of v1, /device:TPU:1, one launch (start us, length us, event | category | flops | bytes accessed | tf_op | source)
XLA Modules:
  0.0 396.4 jit_solution(1212628433073211027)
XLA Ops:
  8.1 51.1 %all-gather.17.cloned.1.call-done = bf16[22528,64]{0,1:T(8,128)(2,1)} async-done(((bf16[1408,64]{0,1:T(8,128)(2,1)}), bf16[22528,64]{0,1:T(8,128)(2,1)}) %all-gather.17.cloned.1.call-update) | async-done | bytes 2883600 | tf_op jit(solution)/shard_map/all_gather | solution.py:85
  59.2 3.8 copy.246
  68.8 102.3 %while.21 = (s32[]{:T(128)}, f32[2,256,128]{2,1,0:T(8,128)S(1)}, f32[2,128]{1,0:T(2,128)S(1)}, f32[2]{0:T(128)S(1)}, f32[8,128,2,256]{1,0,3,2:T(8,128)}, /*index...) while((s32[]{:T(128)}, f32[2,256,128]{2,1,0:T(8,128)S(1)}, ...), condition=%wide.region_6.7_spmd.clone, body=%wide.region_0.6_spmd.clone.sunk | while | flops 59952648 | bytes 4685610 | solution.py:202
  73.0 8.2 %dynamic_update_slice.19 = f32[8,128,2,256]{1,0,3,2:T(8,128)} dynamic-update-slice(f32[8,128,2,256]{1,0,3,2:T(8,128)} %get-tuple-element.428, f32[1,128,2,256]{1,0,3,2:T(1,128)S(1)} %copy.336, s32[]{:T(128)} %get-tuple-element.424, s32[]{:T(128)} %constant.38.clone.1..sunk, s32[]{:T(128)} %constant.38.clone.1..sunk, s32[]{:T(128)} %constant.38.clone.1..sunk) | dynamic-update-slice | bytes 524292 | tf_op jit(solution)/shard_map/while/body/jit(dynamic_update_index_in_dim)/dynamic_update_slice | solution.py:202
  85.8 8.2 %dynamic_update_slice.19 = f32[8,128,2,256]{1,0,3,2:T(8,128)} dynamic-update-slice(f32[8,128,2,256]{1,0,3,2:T(8,128)} %get-tuple-element.428, f32[1,128,2,256]{1,0,3,2:T(1,128)S(1)} %copy.336, s32[]{:T(128)} %get-tuple-element.424, s32[]{:T(128)} %constant.38.clone.1..sunk, s32[]{:T(128)} %constant.38.clone.1..sunk, s32[]{:T(128)} %constant.38.clone.1..sunk) | dynamic-update-slice | bytes 524292 | tf_op jit(solution)/shard_map/while/body/jit(dynamic_update_index_in_dim)/dynamic_update_slice | solution.py:202
  98.6 8.2 %dynamic_update_slice.19 = f32[8,128,2,256]{1,0,3,2:T(8,128)} dynamic-update-slice(f32[8,128,2,256]{1,0,3,2:T(8,128)} %get-tuple-element.428, f32[1,128,2,256]{1,0,3,2:T(1,128)S(1)} %copy.336, s32[]{:T(128)} %get-tuple-element.424, s32[]{:T(128)} %constant.38.clone.1..sunk, s32[]{:T(128)} %constant.38.clone.1..sunk, s32[]{:T(128)} %constant.38.clone.1..sunk) | dynamic-update-slice | bytes 524292 | tf_op jit(solution)/shard_map/while/body/jit(dynamic_update_index_in_dim)/dynamic_update_slice | solution.py:202
  111.4 8.2 %dynamic_update_slice.19 = f32[8,128,2,256]{1,0,3,2:T(8,128)} dynamic-update-slice(f32[8,128,2,256]{1,0,3,2:T(8,128)} %get-tuple-element.428, f32[1,128,2,256]{1,0,3,2:T(1,128)S(1)} %copy.336, s32[]{:T(128)} %get-tuple-element.424, s32[]{:T(128)} %constant.38.clone.1..sunk, s32[]{:T(128)} %constant.38.clone.1..sunk, s32[]{:T(128)} %constant.38.clone.1..sunk) | dynamic-update-slice | bytes 524292 | tf_op jit(solution)/shard_map/while/body/jit(dynamic_update_index_in_dim)/dynamic_update_slice | solution.py:202
  124.2 8.2 %dynamic_update_slice.19 = f32[8,128,2,256]{1,0,3,2:T(8,128)} dynamic-update-slice(f32[8,128,2,256]{1,0,3,2:T(8,128)} %get-tuple-element.428, f32[1,128,2,256]{1,0,3,2:T(1,128)S(1)} %copy.336, s32[]{:T(128)} %get-tuple-element.424, s32[]{:T(128)} %constant.38.clone.1..sunk, s32[]{:T(128)} %constant.38.clone.1..sunk, s32[]{:T(128)} %constant.38.clone.1..sunk) | dynamic-update-slice | bytes 524292 | tf_op jit(solution)/shard_map/while/body/jit(dynamic_update_index_in_dim)/dynamic_update_slice | solution.py:202
  136.9 8.2 %dynamic_update_slice.19 = f32[8,128,2,256]{1,0,3,2:T(8,128)} dynamic-update-slice(f32[8,128,2,256]{1,0,3,2:T(8,128)} %get-tuple-element.428, f32[1,128,2,256]{1,0,3,2:T(1,128)S(1)} %copy.336, s32[]{:T(128)} %get-tuple-element.424, s32[]{:T(128)} %constant.38.clone.1..sunk, s32[]{:T(128)} %constant.38.clone.1..sunk, s32[]{:T(128)} %constant.38.clone.1..sunk) | dynamic-update-slice | bytes 524292 | tf_op jit(solution)/shard_map/while/body/jit(dynamic_update_index_in_dim)/dynamic_update_slice | solution.py:202
  149.7 8.2 %dynamic_update_slice.19 = f32[8,128,2,256]{1,0,3,2:T(8,128)} dynamic-update-slice(f32[8,128,2,256]{1,0,3,2:T(8,128)} %get-tuple-element.428, f32[1,128,2,256]{1,0,3,2:T(1,128)S(1)} %copy.336, s32[]{:T(128)} %get-tuple-element.424, s32[]{:T(128)} %constant.38.clone.1..sunk, s32[]{:T(128)} %constant.38.clone.1..sunk, s32[]{:T(128)} %constant.38.clone.1..sunk) | dynamic-update-slice | bytes 524292 | tf_op jit(solution)/shard_map/while/body/jit(dynamic_update_index_in_dim)/dynamic_update_slice | solution.py:202
  162.6 8.2 %dynamic_update_slice.19 = f32[8,128,2,256]{1,0,3,2:T(8,128)} dynamic-update-slice(f32[8,128,2,256]{1,0,3,2:T(8,128)} %get-tuple-element.428, f32[1,128,2,256]{1,0,3,2:T(1,128)S(1)} %copy.336, s32[]{:T(128)} %get-tuple-element.424, s32[]{:T(128)} %constant.38.clone.1..sunk, s32[]{:T(128)} %constant.38.clone.1..sunk, s32[]{:T(128)} %constant.38.clone.1..sunk) | dynamic-update-slice | bytes 524292 | tf_op jit(solution)/shard_map/while/body/jit(dynamic_update_index_in_dim)/dynamic_update_slice | solution.py:202
  172.5 2.9 all-gather.5
  177.3 12.4 %all-gather.6 = bf16[4,516,128]{2,1,0:T(8,128)(2,1)S(1)} all-gather(bf16[1,516,128]{2,1,0:T(8,128)(2,1)S(1)} %maximum_bitcast_fusion.1), channel_id=3, replica_groups=mesh['sp_0'=4,'sp_1'=4,'sp_2'=2,'tp'=4] {'sp_1'}, dimensions={0}, use_global_device_ids=true | all-gather | bytes 660480 | tf_op jit(solution)/shard_map/all_gather | solution.py:28
  191.1 11.0 %all-gather.7 = bf16[4,516,128]{2,1,0:T(8,128)(2,1)S(1)} all-gather(bf16[1,516,128]{2,1,0:T(8,128)(2,1)S(1)} %maximum_bitcast_fusion.2), channel_id=4, replica_groups=mesh['sp_0'=4,'sp_1'=4,'sp_2'=2,'tp'=4] {'sp_0'}, dimensions={0}, use_global_device_ids=true | all-gather | bytes 660480 | tf_op jit(solution)/shard_map/all_gather | solution.py:28
  212.8 14.4 %all_to_all.24 = bf16[4,256,512]{2,1,0:T(8,128)(2,1)S(1)} all-to-all(bf16[4,256,512]{2,1,0:T(8,128)(2,1)S(1)} %bitcast.614), channel_id=1, replica_groups=mesh['sp_0'=4,'sp_1'=4,'sp_2'=2,'tp'=4] {'tp'}, dimensions={0} | all-to-all | bytes 2097152 | tf_op jit(solution)/shard_map/all_to_all | solution.py:249
  227.7 5.9 %fusion.40 = bf16[256,2048]{1,0:T(8,128)(2,1)S(1)} fusion(bf16[256,2048]{0,1:T(8,128)(2,1)S(1)} %bitcast.607, bf16[2048,2048]{1,0:T(8,128)(2,1)} %all-gather.13.cloned.1.call-done, bf16[256,2048]{1,0:T(8,128)(2,1)S(1)} %copy-done.2), kind=kOutput, calls=%fused_computation.77 | convolution fusion | flops 2149056512 | bytes 11534336 | tf_op jit(solution)/shard_map/dot_general | solution.py:250
  234.7 44.8 %all_to_all.25 = bf16[4,256,2048]{2,1,0:T(8,128)(2,1)S(1)} all-to-all(bf16[4,256,2048]{2,1,0:T(8,128)(2,1)S(1)} %stack.2), channel_id=1, replica_groups=mesh['sp_0'=4,'sp_1'=4,'sp_2'=2,'tp'=4] {'tp'}, dimensions={0} | all-to-all | bytes 8388608 | tf_op jit(solution)/shard_map/all_to_all | solution.py:260
  281.7 10.1 %collective-permute-start = (bf16[2,2048]{1,0:T(2,128)(2,1)S(1)}, bf16[2,2048]{1,0:T(2,128)(2,1)S(1)}, u32[]{:S(2)}, u32[]{:S(2)}) collective-permute-start(bf16[2,2048]{1,0:T(2,128)(2,1)S(1)} %slice.352), channel_id=1, source_target_pairs={{0,4},{4,8},{8,12},{12,16},{16,20},{20,24},{24,28},{28,32},{32,36}... | collective-permute-start | bytes 24584 | tf_op jit(solution)/shard_map/ppermute | solution.py:64
  291.9 7.0 %copy.200 = bf16[16,2,1408,64]{2,3,1,0:T(8,128)(2,1)} copy(bf16[16,2,1408,64]{2,0,1,3:T(8,128)(2,1)} %bitcast.608) | data formatting | bytes 11534336 | tf_op jit(solution)/shard_map/transpose | solution.py:88
  298.9 11.9 %fusion.37 = f32[1026,1408]{1,0:T(8,128)} fusion(bf16[2048,2816]{1,0:T(8,128)(2,1)} %all-gather.15.cloned.1.call-done, bf16[1024,2048]{1,0:T(8,128)(2,1)} %bitcast.611, bf16[2,2048]{1,0:T(2,128)(2,1)S(1)} %collective-permute-done), kind=kOutput, calls=%fused_computation.69 | convolution fusion | flops 5925519360 | bytes 15748096 | tf_op jit(solution)/shard_map/dot_general | solution.py:265
  310.9 8.7 %fusion.33 = f32[1026,1408]{1,0:T(8,128)} fusion(bf16[2048,2816]{1,0:T(8,128)(2,1)S(1)} %copy-done.16, bf16[1024,2048]{1,0:T(8,128)(2,1)S(1)} %bitcast.612, bf16[2,2048]{1,0:T(2,128)(2,1)S(1)} %collective-permute-done), kind=kOutput, calls=%fused_computation.62 | convolution fusion | flops 5925519360 | bytes 15748096 | tf_op jit(solution)/shard_map/dot_general | solution.py:266
  319.6 22.6 %convolution_convert_fusion = bf16[1024,2048]{1,0:T(8,128)(2,1)} fusion(bf16[1408,2048]{0,1:T(8,128)(2,1)} %bitcast.609, f32[1026,1408]{1,0:T(8,128)} %fusion.33, f32[1026,1408]{1,0:T(8,128)} %fusion.37, f32[1408]{0:T(1024)S(1)} %get-tuple-element.181, f32[1408]{0:T(1024)S(1)} %get-tuple-element.182, f32[1408]{0:T(1024)S(1)} %get-tuple-element.180, ...), kind=kOutput, calls=%fused_computation.72 | convolution fusion | flops 5930745856 | bytes 44598272 | tf_op jit(solution)/shard_map/dot_general | solution.py:280
  342.2 45.0 %reduce-scatter.2.cloned.1.call-done = bf16[256,2048]{1,0:T(8,128)(2,1)} async-done(((bf16[1024,2048]{1,0:T(8,128)(2,1)}), bf16[256,2048]{1,0:T(8,128)(2,1)}) %reduce-scatter.2.cloned.1.call-update) | async-done | bytes 1048592 | tf_op jit(solution)/shard_map/reduce_scatter | solution.py:279
  387.2 2.6 fusion.44
  (370 shorter events, 61.9 us)
Async XLA Ops:
  6.5 52.6 %all-gather.17.cloned.1.call-start = ((), (), s32[]{:S(2)}) async-start(), calls=%async_computation.6 | async-start | bytes 3063808 | tf_op jit(solution)/shard_map/all_gather | solution.py:85
  7.3 220.4 %all-gather.13.cloned.1.call-start = ((), (), s32[]{:S(2)}) async-start(), calls=%async_computation.3 | async-start | bytes 10485760 | tf_op jit(solution)/shard_map/all_gather | solution.py:248
  8.0 283.9 %all-gather.19.cloned.1.call-start = ((), (), s32[]{:S(2)}) async-start(), calls=%async_computation.7 | async-start | bytes 8650752 | tf_op jit(solution)/shard_map/all_gather | solution.py:85
  59.1 3.9 copy-start.7
  59.2 3.9 copy-start.8
  59.2 4.9 %copy-start.12 = (f32[1024,2]{0,1:T(2,128)S(1)}, f32[1024,2]{0,1:T(2,128)}, u32[]{:S(2)}) copy-start(f32[1024,2]{0,1:T(2,128)} %param.25) | copy-start | bytes 24580
  59.2 4.9 %copy-start.13 = (f32[1024,2]{0,1:T(2,128)S(1)}, f32[1024,2]{0,1:T(2,128)}, u32[]{:S(2)}) copy-start(f32[1024,2]{0,1:T(2,128)} %param.24) | copy-start | bytes 24580
  63.0 2.7 copy-start.14
  63.0 2.9 copy-start.3
  63.0 235.9 %all-gather.15.cloned.1.call-start = ((), (), s32[]{:S(2)}) async-start(), calls=%async_computation.4 | async-start | bytes 11894784 | tf_op jit(solution)/shard_map/all_gather | solution.py:69
  63.9 323.3 %reduce-scatter.2.cloned.1.call-start = ((), (), s32[]{:S(2)}) async-start(), calls=%async_computation.5 | async-start | bytes 5242880 | tf_op jit(solution)/shard_map/reduce_scatter | solution.py:279
  171.1 31.0 %copy-start.6 = (f32[8,128,2]{2,1,0:T(8,128)S(1)}, f32[8,128,2]{2,1,0:T(8,128)}, u32[]{:S(2)}) copy-start(f32[8,128,2]{2,1,0:T(8,128)} %get-tuple-element.72) | copy-start | bytes 24580
  171.1 31.2 %copy-start.5 = (f32[8,128,2]{2,1,0:T(8,128)S(1)}, f32[8,128,2]{2,1,0:T(8,128)}, u32[]{:S(2)}) copy-start(f32[8,128,2]{2,1,0:T(8,128)} %get-tuple-element.77) | copy-start | bytes 24580
  204.3 2.6 copy-start.4
  206.8 1.3 copy-start.15
  210.2 17.4 %copy-start.2 = (bf16[256,2048]{1,0:T(8,128)(2,1)S(1)}, bf16[256,2048]{1,0:T(8,128)(2,1)}, u32[]{:S(2)}) copy-start(bf16[256,2048]{1,0:T(8,128)(2,1)} %param.18) | copy-start | bytes 3145732
  227.7 6.2 %copy-start.11 = (f32[2048]{0:T(1024)S(1)}, f32[2048]{0:T(1024)}, u32[]{:S(2)}) copy-start(f32[2048]{0:T(1024)} %param.28) | copy-start | bytes 24580
  234.7 57.0 %copy-start.9 = (f32[3,1408]{1,0:T(4,128)S(1)}, f32[3,1408]{1,0:T(4,128)}, u32[]{:S(2)}) copy-start(f32[3,1408]{1,0:T(4,128)} %param.32) | copy-start | bytes 50692
  234.7 57.0 %copy-start.10 = (f32[3,1408]{1,0:T(4,128)S(1)}, f32[3,1408]{1,0:T(4,128)}, u32[]{:S(2)}) copy-start(f32[3,1408]{1,0:T(4,128)} %param.31) | copy-start | bytes 50692
  279.6 2.1 copy-start
  281.7 17.3 %collective-permute-start = (bf16[2,2048]{1,0:T(2,128)(2,1)S(1)}, bf16[2,2048]{1,0:T(2,128)(2,1)S(1)}, u32[]{:S(2)}, u32[]{:S(2)}) collective-permute-start(bf16[2,2048]{1,0:T(2,128)(2,1)S(1)} %slice.352), channel_id=1, source_target_pairs={{0,4},{4,8},{8,12},{12,16},{16,20},{20,24},{24,28},{28,32},{32,36}... | collective-permute-start | bytes 24584 | tf_op jit(solution)/shard_map/ppermute | solution.py:64
  298.9 12.0 %copy-start.1 = (bf16[4,256,2048]{2,1,0:T(8,128)(2,1)S(1)}, bf16[4,256,2048]{2,1,0:T(8,128)(2,1)}, u32[]{:S(2)}) copy-start(bf16[4,256,2048]{2,1,0:T(8,128)(2,1)} %copy-done) | copy-start | bytes 12582916
  298.9 12.0 %copy-start.16 = (bf16[2048,2816]{1,0:T(8,128)(2,1)S(1)}, bf16[2048,2816]{1,0:T(8,128)(2,1)}, u32[]{:S(2)}) copy-start(bf16[2048,2816]{1,0:T(8,128)(2,1)} %all-gather.15.cloned.1.call-done) | copy-start | bytes 34603012
Sparse Core Ops, SparseCore 0:
  9.5 49.5 all-gather.16
  60.8 82.5 all-gather.12
  145.1 20.1 all-gather.18
  167.4 63.4 all-gather.14
  342.4 44.8 reduce-scatter.1
